TPU v7x, 32 devices: a whole 2x2x4 slice. The times are simulated.
32 devices in a mesh: sp: 8 (over z, x), dp: 4 (over y, core).
Axes of the slice: x: 2, y: 2, z: 4, core: 2. Of those that a mesh axis runs over, the one named last changes fastest.
Arguments:
- queries: bfloat16 [4, 1024, 2048], P('dp', 'sp'), may hold values from -12 to 12
- key_rows: bfloat16 [4, 1024, 2048], P('dp', 'sp'), may hold values from -12 to 12
- value_rows: bfloat16 [4, 1024, 2048], P('dp', 'sp'), may hold values from -6 to 6
- lambdas: float32 [16], P('sp'), may hold values from 0.3 to 0.8
- head_gain: float32 [128], replicated, may hold values from 0.1 to 1.9
- out_weight: bfloat16 [2048, 2048], replicated, may hold values from -0.125 to 0.125
- residual: bfloat16 [4, 1024, 2048], P('dp', 'sp'), may hold values from -6 to 6
- mixer_gain: float32 [2048], replicated, may hold values from 0.1 to 1.9
- channel_gain: float32 [2048], replicated, may hold values from 0.1 to 1.9
- expert_gain: float32 [2048], replicated, may hold values from 0.1 to 1.9
- routes: int32 [4, 1024, 2], P('dp', 'sp'), may hold values from 0 to 7, all different within a row; in each aligned block of 128 rows (0 to 127, 128 to 255, ..., all dimensions but the last counted through in order) at most 48 rows name the same one
- route_logits: float32 [4, 1024, 2], P('dp', 'sp'), may hold values from -5 to 5
- gate_weight: bfloat16 [8, 2048, 4096], P('sp', None, 'dp'), may hold values from -0.125 to 0.125
- up_weight: bfloat16 [8, 2048, 4096], P('sp', None, 'dp'), may hold values from -0.125 to 0.125
- down_weight: bfloat16 [8, 4096, 2048], P('sp', 'dp'), may hold values from -0.09375 to 0.09375
Outputs:
- updated: bfloat16 [4, 1024, 2048], P('dp', 'sp')
Inputs may be any that keep to these rules, and one draw needn't show every extreme that they name: `routes`: among the rows of one device no expert is named by more than 48 rows; in some of these blocks one expert is named by exactly 48.
All inputs are finite; a program needn't handle non-finite values.
Results may differ from a plain program's by a relative error of at most 0.014.
Values may be sent and summed in bfloat16 or wider, within the bound.
A program may use at most 128 MiB of HBM per device.

v0:
```python
import math
import jax
import jax.numpy as jnp
from jax import lax
from jax.sharding import PartitionSpec as P


def rotate(field):
    dim_full = field.shape[-1]
    dim_half = dim_full // 2
    inverse = 1.0 / 10000.0 ** (jnp.arange(0, dim_full, 2, dtype=jnp.float32) / dim_full)
    angles = jnp.arange(field.shape[-4], dtype=jnp.float32)[:, None] * inverse[None, :]
    cosine = jnp.cos(angles)[:, None, None, :]
    sine_table = jnp.sin(angles)[:, None, None, :]
    floats = field.astype(jnp.float32)
    front_part = floats[..., :dim_half]
    second = floats[..., dim_half:]
    turned = jnp.concatenate(
        [front_part * cosine - second * sine_table, second * cosine + front_part * sine_table],
        axis=-1,
    )
    return turned.astype(jnp.bfloat16)


def rms_scale(values, epsilon):
    return values * lax.rsqrt(jnp.mean(values * values, axis=-1, keepdims=True) + epsilon)


def local(
    queries,
    key_rows,
    value_rows,
    lambdas,
    head_gain,
    out_weight,
    residual,
    mixer_gain,
    channel_gain,
    expert_gain,
    routes,
    route_logits,
    gate_weight,
    up_weight,
    down_weight,
):
    head_count = lambdas.shape[0]
    head_dim = head_gain.shape[0] // 2
    seq_query, seq_keys, seq_values = (
        lax.all_to_all(queries, "sp", split_axis=2, concat_axis=1, tiled=True),
        lax.all_to_all(key_rows, "sp", split_axis=2, concat_axis=1, tiled=True),
        lax.all_to_all(value_rows, "sp", split_axis=2, concat_axis=1, tiled=True),
    )
    length = seq_query.shape[1]
    query_rot = rotate(seq_query.reshape(length, head_count, 2, head_dim))
    keys_rot = rotate(seq_keys.reshape(length, head_count, 2, head_dim))
    values_heads = seq_values.reshape(length, head_count, 2 * head_dim)
    block_rows = math.gcd(length, 256)
    query_blocks = query_rot.reshape(length // block_rows, block_rows, head_count, 2, head_dim)
    scale = head_dim ** (-0.5)

    def one_block(query_block):
        scores = (
            jnp.einsum("qhcd,khcd->hcqk", query_block, keys_rot, preferred_element_type=jnp.float32)
            * scale
        )
        probs = jax.nn.softmax(scores, axis=-1)
        mixing = (probs[:, 0] - lambdas[:, None, None] * probs[:, 1]).astype(jnp.bfloat16)
        head_mix = jnp.einsum(
            "hqk,khv->qhv", mixing, values_heads, preferred_element_type=jnp.float32
        )
        return (rms_scale(head_mix, 1e-05) * head_gain).astype(jnp.bfloat16)

    head_out = lax.map(one_block, query_blocks).reshape(1, length, head_count * 2 * head_dim)
    token_rows = lax.all_to_all(head_out, "sp", split_axis=1, concat_axis=2, tiled=True)
    tokens = residual.shape[1]
    model_dim = residual.shape[2]
    projected = jnp.dot(
        token_rows.reshape(tokens, -1), out_weight, preferred_element_type=jnp.float32
    )
    stream = (
        residual.reshape(tokens, model_dim).astype(jnp.float32)
        + rms_scale(projected, 1e-06) * mixer_gain
    ).astype(jnp.bfloat16)
    normed = (rms_scale(stream.astype(jnp.float32), 1e-06) * channel_gain).astype(jnp.bfloat16)
    sp_count = lax.axis_size("sp")
    expert_count = sp_count * gate_weight.shape[0]
    capacity = max(2, 3 * tokens // expert_count)
    top_count = routes.shape[2]
    choice_ids = routes.reshape(-1)
    slots_all = choice_ids.shape[0]
    one_hot = (choice_ids[:, None] == jnp.arange(expert_count, dtype=jnp.int32)[None, :]).astype(
        jnp.int32
    )
    running = jnp.cumsum(one_hot, axis=0)
    slot_index = jnp.sum(one_hot * running, axis=1) - 1
    target = choice_ids * capacity + slot_index
    source_rows = jnp.arange(slots_all, dtype=jnp.int32) // top_count
    outgoing = (
        jnp.zeros((expert_count * capacity, model_dim), jnp.bfloat16)
        .at[target]
        .set(normed[source_rows])
    )
    outgoing = outgoing.reshape(expert_count, capacity, model_dim)
    arrived = lax.all_to_all(outgoing, "sp", split_axis=0, concat_axis=0, tiled=True).reshape(
        sp_count, 1, capacity, model_dim
    )
    expert_arrived = lax.all_gather(arrived, "dp", axis=1, tiled=True)
    shape_in = expert_arrived.shape
    flat_rows = expert_arrived.reshape(-1, shape_in[-1])
    gate_act = jnp.dot(flat_rows, gate_weight[0], preferred_element_type=jnp.float32)
    up_act = jnp.dot(flat_rows, up_weight[0], preferred_element_type=jnp.float32)
    hidden = (jax.nn.silu(gate_act) * up_act).astype(jnp.bfloat16)
    part = jnp.dot(hidden, down_weight[0], preferred_element_type=jnp.float32).astype(jnp.bfloat16)
    partial_value = part.reshape(shape_in)
    summed = lax.psum_scatter(
        partial_value.astype(jnp.float32).astype(jnp.bfloat16),
        "dp",
        scatter_dimension=1,
        tiled=True,
    )
    returned = lax.all_to_all(summed, "sp", split_axis=0, concat_axis=0, tiled=True).reshape(
        expert_count * capacity, model_dim
    )
    picked = returned[target].astype(jnp.float32).reshape(tokens, top_count, model_dim)
    shares = jax.nn.softmax(route_logits.reshape(tokens, top_count), axis=-1)
    combined = jnp.sum(picked * shares[:, :, None], axis=1)
    updated = stream.astype(jnp.float32) + rms_scale(combined, 1e-06) * expert_gain
    return updated.astype(jnp.bfloat16).reshape(1, tokens, model_dim)


def solution(mesh):
    placed = (
        P("dp", "sp", None),
        P("dp", "sp", None),
        P("dp", "sp", None),
        P("sp"),
        P(),
        P(),
        P("dp", "sp", None),
        P(),
        P(),
        P(),
        P("dp", "sp", None),
        P("dp", "sp", None),
        P("sp", None, "dp"),
        P("sp", None, "dp"),
        P("sp", "dp", None),
    )
    return jax.shard_map(
        local, mesh=mesh, in_specs=placed, out_specs=P("dp", "sp", None), check_vma=False
    )
```

profile of v0, /device:TPU:0, one launch (start us, length us, event | category | flops | bytes accessed | tf_op | source)
XLA Modules:
  0.0 459.4 jit_solution(8292478884959336948)
XLA Ops:
  6.5 2.4 copy.66
  9.5 11.5 %reduce.4 = bf16[2048,128]{1,0:T(8,128)(2,1)S(1)} reduce(bf16[2048,1,128]{2,1,0:T(2,128)(2,1)S(1)} %bitcast.147, bf16[]{:T(256)} %broadcast.286), dimensions={1}, to_apply=%bitcast.104.reduce_sub_computation | reduce | bytes 1048578
  22.0 7.3 %all-to-all-start = ((bf16[8,2,16384]{2,1,0:T(2,128)(2,1)}), bf16[8,2,16384]{2,1,0:T(2,128)(2,1)S(1)}, u32[]{:S(2)}, u32[]{:S(2)}) async-start(bf16[8,2,16384]{2,1,0:T(2,128)(2,1)} %reshape.320), calls=%async_computation | async-start | bytes 1048576 | tf_op jit(solution)/shard_map/all_to_all | solution.py:49
  30.0 11.5 %reduce.3 = bf16[2048,128]{1,0:T(8,128)(2,1)S(1)} reduce(bf16[2048,1,128]{2,1,0:T(2,128)(2,1)S(1)} %bitcast.151, bf16[]{:T(256)} %broadcast.286), dimensions={1}, to_apply=%bitcast.106.reduce_sub_computation | reduce | bytes 1048578
  43.7 16.1 %all-to-all-start.1 = ((bf16[8,2,16384]{2,1,0:T(2,128)(2,1)}), bf16[8,2,16384]{2,1,0:T(2,128)(2,1)S(1)}, u32[]{:S(2)}, u32[]{:S(2)}) async-start(bf16[8,2,16384]{2,1,0:T(2,128)(2,1)} %reshape.322), calls=%async_computation.1 | async-start | bytes 1048576 | tf_op jit(solution)/shard_map/all_to_all | solution.py:50
  60.6 11.5 %reduce.5 = bf16[2048,128]{1,0:T(8,128)(2,1)S(1)} reduce(bf16[2048,1,128]{2,1,0:T(2,128)(2,1)S(1)} %bitcast.152, bf16[]{:T(256)} %broadcast.286), dimensions={1}, to_apply=%bitcast.108.reduce_sub_computation | reduce | bytes 1048578
  73.9 6.0 %all-to-all-start.2 = ((bf16[8,2,16384]{2,1,0:T(2,128)(2,1)}), bf16[8,2,16384]{2,1,0:T(2,128)(2,1)}, u32[]{:S(2)}, u32[]{:S(2)}) async-start(bf16[8,2,16384]{2,1,0:T(2,128)(2,1)} %reshape.324), calls=%async_computation.2 | async-start | bytes 1048576 | tf_op jit(solution)/shard_map/all_to_all | solution.py:51
  85.8 7.6 %all-to-all-done.2 = bf16[8,2,16384]{2,1,0:T(2,128)(2,1)} async-done(((bf16[8,2,16384]{2,1,0:T(2,128)(2,1)}), bf16[8,2,16384]{2,1,0:T(2,128)(2,1)}, u32[]{:S(2)}, u32[]{:S(2)}) %all-to-all-start.2) | async-done | bytes 524320 | tf_op jit(solution)/shard_map/all_to_all | solution.py:51
  98.1 27.5 %while.10 = (s32[]{:T(128)}, bf16[4,256,2,128]{3,2,1,0:T(2,128)(2,1)S(1)}, bf16[4,256,2,2,64]{1,4,3,2,0:T(8,128)(2,1)S(1)}, bf16[1024,2,2,64]{0,3,2,1:T(8,128)(2...) while((s32[]{:T(128)}, ...), condition=%wide.region_4.5_spmd, body=%wide.region_0.4_spmd.sunk | while | flops 274531840 | bytes 19153508 | solution.py:73
  98.1 3.3 fusion.74
  101.4 2.6 broadcast_divide_fusion.2
  105.0 3.3 fusion.74
  108.3 2.6 broadcast_divide_fusion.2
  111.8 3.3 fusion.74
  115.1 2.6 broadcast_divide_fusion.2
  118.7 3.3 fusion.74
  122.0 2.6 broadcast_divide_fusion.2
  125.8 3.8 reduce.6
  130.5 3.7 all-to-all-start.3
  134.9 13.1 %all-to-all-done.3 = bf16[8,2,16384]{2,1,0:T(2,128)(2,1)S(1)} async-done(((bf16[8,2,16384]{2,1,0:T(2,128)(2,1)}), bf16[8,2,16384]{2,1,0:T(2,128)(2,1)S(1)}, u32[]{:S(2)}, u32[]{:S(2)}) %all-to-all-start.3) | async-done | bytes 524320 | tf_op jit(solution)/shard_map/all_to_all | solution.py:74
  148.9 4.8 %multiply_reduce_fusion.4 = (f32[128]{0:T(128)S(1)}, f32[128,2048]{1,0:T(8,128)S(1)}) fusion(bf16[128,2048]{0,1:T(8,128)(2,1)S(1)} %bitcast.153, bf16[2048,2048]{1,0:T(8,128)(2,1)} %param.22), kind=kOutput, calls=%fused_computation.50 | convolution fusion | flops 1074265984 | bytes 9961984 | tf_op jit(solution)/shard_map/dot_general | solution.py:77
  154.3 5.9 %scatter_custom_fusion = bf16[384,2048]{1,0:T(8,128)(2,1)S(1)} fusion(s32[256]{0:T(256)S(1)} %bitcast.158, bf16[128,2048]{1,0:T(8,128)(2,1)S(1)} %fusion.38, s32[1024]{0:T(1024)S(1)} %pad_clamp_fusion.1, bf16[]{:T(256)} %constant.64.clone.1), kind=kCustom, calls=%fused_computation.47 | custom fusion | bytes 1572866 | tf_op jit(solution)/shard_map/scatter | solution.py:101
  160.3 39.9 %all_to_all.58 = bf16[8,48,2048]{2,1,0:T(8,128)(2,1)} all-to-all(bf16[8,48,2048]{2,1,0:T(8,128)(2,1)S(1)} %bitcast.144), channel_id=1, replica_groups=mesh['sp'=8,'dp'=4] {'sp'}, dimensions={0} | all-to-all | bytes 3145728 | tf_op jit(solution)/shard_map/all_to_all | solution.py:104
  200.6 45.1 %all-gather.3.cloned.1.call-done = bf16[8,192,2048]{2,1,0:T(8,128)(2,1)} async-done(((bf16[8,48,2048]{2,1,0:T(8,128)(2,1)}), bf16[8,192,2048]{2,1,0:T(8,128)(2,1)}) %all-gather.3.cloned.1.call-update) | async-done | bytes 6291472 | tf_op jit(solution)/shard_map/all_gather | solution.py:107
  245.7 11.6 %fusion.33 = f32[1536,1024]{1,0:T(8,128)} fusion(bf16[1536,2048]{1,0:T(8,128)(2,1)} %bitcast.162, bf16[1,2048,1024]{2,1,0:T(8,128)(2,1)} %param.29), kind=kOutput, calls=%fused_computation.34 | convolution fusion | flops 6442450944 | bytes 16777216 | tf_op jit(solution)/shard_map/dot_general | solution.py:110
  257.3 20.5 %convolution_convert_fusion = bf16[1536,2048]{1,0:T(8,128)(2,1)} fusion(bf16[1,1024,2048]{2,1,0:T(8,128)(2,1)} %param.31, f32[1536,1024]{1,0:T(8,128)} %fusion.33, bf16[1536,2048]{1,0:T(8,128)(2,1)} %bitcast.163, bf16[1,2048,1024]{2,1,0:T(8,128)(2,1)} %param.30), kind=kOutput, calls=%fused_computation.30 | convolution fusion | flops 12897484800 | bytes 27262976 | tf_op jit(solution)/shard_map/dot_general | solution.py:113
  279.1 118.5 %all-reduce.3.cloned.1.call-done = bf16[8,4,48,2048]{3,2,1,0:T(8,128)(2,1)} async-done(((bf16[8,4,48,2048]{3,2,1,0:T(8,128)(2,1)}), bf16[8,4,48,2048]{3,2,1,0:T(8,128)(2,1)}) %all-reduce.3.cloned.1.call-update) | async-done | bytes 6291472
  397.6 3.4 constant_dynamic-slice_fusion
  401.0 5.7 %all-to-all-start.5 = ((bf16[8,1,48,2048]{3,2,1,0:T(8,128)(2,1)}), bf16[8,1,48,2048]{3,2,1,0:T(8,128)(2,1)S(1)}, u32[]{:S(2)}, u32[]{:S(2)}) async-start(bf16[8,1,48,2048]{3,2,1,0:T(8,128)(2,1)} %constant_dynamic-slice_fusion), calls=%async_computation.5 | async-start | bytes 3145728 | tf_op jit(solution)/shard_map/all_to_all | solution.py:121
  406.9 36.4 %all-to-all-done.5 = bf16[8,1,48,2048]{3,2,1,0:T(8,128)(2,1)S(1)} async-done(((bf16[8,1,48,2048]{3,2,1,0:T(8,128)(2,1)}), bf16[8,1,48,2048]{3,2,1,0:T(8,128)(2,1)S(1)}, u32[]{:S(2)}, u32[]{:S(2)}) %all-to-all-start.5) | async-done | bytes 1572896 | tf_op jit(solution)/shard_map/all_to_all | solution.py:121
  445.6 2.4 reshape.280
  448.0 3.2 multiply_reduce_fusion.2
  (115 shorter events, 29.7 us)
Async XLA Ops:
  6.5 22.7 %copy-start = (bf16[1,128,2048]{2,1,0:T(8,128)(2,1)S(1)}, bf16[1,128,2048]{2,1,0:T(8,128)(2,1)}, u32[]{:S(2)}) copy-start(bf16[1,128,2048]{2,1,0:T(8,128)(2,1)} %param.18) | copy-start | bytes 1572868
  9.5 50.3 %copy-start.1 = (bf16[1,128,2048]{2,1,0:T(8,128)(2,1)S(1)}, bf16[1,128,2048]{2,1,0:T(8,128)(2,1)}, u32[]{:S(2)}) copy-start(bf16[1,128,2048]{2,1,0:T(8,128)(2,1)} %param.19) | copy-start | bytes 1572868
  22.0 21.8 %all-to-all-start = ((bf16[8,2,16384]{2,1,0:T(2,128)(2,1)}), bf16[8,2,16384]{2,1,0:T(2,128)(2,1)S(1)}, u32[]{:S(2)}, u32[]{:S(2)}) async-start(bf16[8,2,16384]{2,1,0:T(2,128)(2,1)} %reshape.320), calls=%async_computation | async-start | bytes 1048576 | tf_op jit(solution)/shard_map/all_to_all | solution.py:49
  30.0 43.0 %copy-start.11 = (s32[1,128,2]{1,2,0:T(2,128)S(1)}, s32[1,128,2]{1,2,0:T(2,128)}, u32[]{:S(2)}) copy-start(s32[1,128,2]{1,2,0:T(2,128)} %param.27) | copy-start | bytes 3076
  43.7 30.1 %all-to-all-start.1 = ((bf16[8,2,16384]{2,1,0:T(2,128)(2,1)}), bf16[8,2,16384]{2,1,0:T(2,128)(2,1)S(1)}, u32[]{:S(2)}, u32[]{:S(2)}) async-start(bf16[8,2,16384]{2,1,0:T(2,128)(2,1)} %reshape.322), calls=%async_computation.1 | async-start | bytes 1048576 | tf_op jit(solution)/shard_map/all_to_all | solution.py:50
  73.9 19.5 %all-to-all-start.2 = ((bf16[8,2,16384]{2,1,0:T(2,128)(2,1)}), bf16[8,2,16384]{2,1,0:T(2,128)(2,1)}, u32[]{:S(2)}, u32[]{:S(2)}) async-start(bf16[8,2,16384]{2,1,0:T(2,128)(2,1)} %reshape.324), calls=%async_computation.2 | async-start | bytes 1048576 | tf_op jit(solution)/shard_map/all_to_all | solution.py:51
  80.3 3.6 copy-start.10
  95.6 1.9 copy-start.2
  95.7 1.9 copy-start.5
  95.7 1.9 copy-start.12
  97.0 1.0 copy-start.3
  125.5 9.2 %slice-start = ((s32[8,3]{0,1:T(4,128)}), s32[8,2]{0,1:T(2,128)S(1)}, s32[]{:S(2)}) async-start(s32[8,3]{0,1:T(4,128)} %copy-done.10), calls=%async_computation.8 | async-start | bytes 2048 | tf_op jit(solution)/shard_map/slice.1
  130.5 17.5 %all-to-all-start.3 = ((bf16[8,2,16384]{2,1,0:T(2,128)(2,1)}), bf16[8,2,16384]{2,1,0:T(2,128)(2,1)S(1)}, u32[]{:S(2)}, u32[]{:S(2)}) async-start(bf16[8,2,16384]{2,1,0:T(2,128)(2,1)} %reshape.326), calls=%async_computation.3 | async-start | bytes 1048576 | tf_op jit(solution)/shard_map/all_to_all | solution.py:74
  134.2 111.5 %all-gather.3.cloned.1.call-start = ((), (), s32[]{:S(2)}) async-start(), calls=%async_computation.6 | async-start | bytes 7864320 | tf_op jit(solution)/shard_map/all_gather | solution.py:107
  148.9 4.8 %copy-start.4 = (bf16[1,128,2048]{2,1,0:T(8,128)(2,1)S(1)}, bf16[1,128,2048]{2,1,0:T(8,128)(2,1)}, u32[]{:S(2)}) copy-start(bf16[1,128,2048]{2,1,0:T(8,128)(2,1)} %param.23) | copy-start | bytes 1572868
  148.9 4.8 %copy-start.7 = (f32[2048]{0:T(1024)S(1)}, f32[2048]{0:T(1024)}, u32[]{:S(2)}) copy-start(f32[2048]{0:T(1024)} %param.24) | copy-start | bytes 24580
  148.9 5.2 %copy-start.8 = (f32[2048]{0:T(1024)S(1)}, f32[2048]{0:T(1024)}, u32[]{:S(2)}) copy-start(f32[2048]{0:T(1024)} %param.25) | copy-start | bytes 24580
  200.2 197.4 %all-reduce.3.cloned.1.call-start = ((), (), s32[]{:S(2)}) async-start(), calls=%async_computation.7 | async-start | bytes 12582912
  277.9 0.7 copy-start.13
  277.9 128.8 %copy-start.6 = (f32[1,128,2]{1,2,0:T(2,128)S(1)}, f32[1,128,2]{1,2,0:T(2,128)}, u32[]{:S(2)}) copy-start(f32[1,128,2]{1,2,0:T(2,128)} %param.28) | copy-start | bytes 3076
  401.0 42.3 %all-to-all-start.5 = ((bf16[8,1,48,2048]{3,2,1,0:T(8,128)(2,1)}), bf16[8,1,48,2048]{3,2,1,0:T(8,128)(2,1)S(1)}, u32[]{:S(2)}, u32[]{:S(2)}) async-start(bf16[8,1,48,2048]{3,2,1,0:T(8,128)(2,1)} %constant_dynamic-slice_fusion), calls=%async_computation.5 | async-start | bytes 3145728 | tf_op jit(solution)/shard_map/all_to_all | solution.py:121
  445.6 5.7 %copy-start.9 = (f32[2048]{0:T(1024)S(1)}, f32[2048]{0:T(1024)}, u32[]{:S(2)}) copy-start(f32[2048]{0:T(1024)} %param.26) | copy-start | bytes 24580
Sparse Core Ops, SparseCore 0:
  200.3 45.3 all-gather.2
  278.0 119.5 all-reduce.2
where the time goes:
time: 468 us; the launch traced here: 459 us
  waiting for transfers between devices  222 us (47%)
  other arithmetic  58.1 us (12%)
  matrix products  52.5 us (11%)
  blocking collectives  39.9 us (9%)
  starting transfers between devices  39.5 us (8%)
  local copies, waits for them, and re-layouts  33.3 us (7%)
  between operations  14.1 us (3%)
    unnamed x3, waiting for transfers between devices  119 us
    all_gather x1, waiting for transfers between devices, local(): expert_arrived = lax.all_gather(arrived, 'dp', axis=1, tiled=True)  45.1 us
    all_to_all x1, blocking collectives, local(): lax.all_to_all(outgoing, 'sp', split_axis=0, concat_axis=0, tiled=True)  39.9 us
    unnamed x4, other arithmetic  38.3 us
    all_to_all x1, waiting for transfers between devices, local(): lax.all_to_all(summed, 'sp', split_axis=0, concat_axis=0, tiled=True)  36.4 us
    dot_general x1, matrix products, local(): jnp.dot(hidden, down_weight[0], preferred_element_type=jnp.float32)  20.5 us
    unnamed x45, local copies, waits for them, and re-layouts  17.4 us
    all_to_all x1, starting transfers between devices, local(): lax.all_to_all(key_rows, 'sp', split_axis=2, concat_axis=1, tiled=True)  16.1 us
  transfers between devices with their start and end apart: 7, of which 6 were waited for; matrix products, arithmetic and copies ran while one was open for 7% of the time, Pallas kernels for 0%

commit v1 on v0

--- a/solution.py
+++ b/solution.py
@@ -104,7 +104,12 @@
     arrived = lax.all_to_all(outgoing, "sp", split_axis=0, concat_axis=0, tiled=True).reshape(
         sp_count, 1, capacity, model_dim
     )
-    expert_arrived = lax.all_gather(arrived, "dp", axis=1, tiled=True)
+    ring = [arrived]
+    for hop in range(3):
+        ring.append(lax.ppermute(ring[-1], "dp", [(dev, (dev + 1) % 4) for dev in range(4)]))
+    expert_arrived = jnp.roll(
+        jnp.concatenate(ring[::-1], axis=1), (lax.axis_index("dp") + 1) * ring[0].shape[1], axis=1
+    )
     shape_in = expert_arrived.shape
     flat_rows = expert_arrived.reshape(-1, shape_in[-1])
     gate_act = jnp.dot(flat_rows, gate_weight[0], preferred_element_type=jnp.float32)

time: 468 us -> 499 us (1.066)
  local copies, waits for them, and re-layouts: 33.3 us -> 59.8 us
  waiting for transfers between devices: 222 us -> 236 us
  starting transfers between devices: 39.5 us -> 28.2 us
    ppermute x0 -> x3, waiting for transfers between devices: none -> 59.9 us  [local(): lax.ppermute(ring[-1], 'dp', [(dev, (dev + 1) % 4) for dev in range(4)])]
    all_gather x1 -> x0, waiting for transfers between devices: 45.1 us -> none  [local(): expert_arrived = lax.all_gather(arrived, 'dp', axis=1, tiled=True)]
    unnamed x45 -> x60, local copies, waits for them, and re-layouts: 17.4 us -> 35.7 us
    all_to_all x1, starting transfers between devices: 16.1 us -> 4.93 us  [local(): lax.all_to_all(key_rows, 'sp', split_axis=2, concat_axis=1, tiled=True)]
    unnamed x3 -> x2, waiting for transfers between devices: 119 us -> 118 us
  transfers between devices with their start and end apart: 7 -> 9, of which waited for: 6 -> 8; matrix products, arithmetic and copies ran while one was open for 7% -> 7% of each run, Pallas kernels for 0% -> 0%
where the time goes in v1:
time: 499 us; the launch traced here: 490 us
  waiting for transfers between devices  236 us (47%)
  local copies, waits for them, and re-layouts  59.8 us (12%)
  other arithmetic  58.2 us (12%)
  matrix products  53.5 us (11%)
  blocking collectives  39.8 us (8%)
  starting transfers between devices  28.2 us (6%)
  between operations  14.1 us (3%)
    unnamed x2, waiting for transfers between devices  118 us
    ppermute x3, waiting for transfers between devices, local(): lax.ppermute(ring[-1], 'dp', [(dev, (dev + 1) % 4) for dev in range(4)])  59.9 us
    all_to_all x1, blocking collectives, local(): lax.all_to_all(outgoing, 'sp', split_axis=0, concat_axis=0, tiled=True)  39.8 us
    unnamed x4, other arithmetic  38.4 us
    all_to_all x1, waiting for transfers between devices, local(): lax.all_to_all(summed, 'sp', split_axis=0, concat_axis=0, tiled=True)  36.4 us
    unnamed x60, local copies, waits for them, and re-layouts  35.7 us
    dot_general x1, matrix products, local(): jnp.dot(hidden, down_weight[0], preferred_element_type=jnp.float32)  20.6 us
    sub x4, matrix products, one_block(): probs = jax.nn.softmax(scores, axis=-1)  13.2 us
  transfers between devices with their start and end apart: 9, of which 8 were waited for; matrix products, arithmetic and copies ran while one was open for 7% of the time, Pallas kernels for 0%

profile of v1, /device:TPU:0, one launch (start us, length us, event | category | flops | bytes accessed | tf_op | source)
XLA Modules:
  0.0 489.9 jit_solution(8319201706557502002)
XLA Ops:
  9.5 11.6 %reduce.4 = bf16[2048,128]{1,0:T(8,128)(2,1)S(1)} reduce(bf16[2048,1,128]{2,1,0:T(2,128)(2,1)S(1)} %bitcast.153, bf16[]{:T(256)} %broadcast.287), dimensions={1}, to_apply=%bitcast.107.reduce_sub_computation | reduce | bytes 1048578
  22.0 7.3 %all-to-all-start = ((bf16[8,2,16384]{2,1,0:T(2,128)(2,1)}), bf16[8,2,16384]{2,1,0:T(2,128)(2,1)S(1)}, u32[]{:S(2)}, u32[]{:S(2)}) async-start(bf16[8,2,16384]{2,1,0:T(2,128)(2,1)} %reshape.318), calls=%async_computation | async-start | bytes 1048576 | tf_op jit(solution)/shard_map/all_to_all | solution.py:49
  30.1 11.5 %reduce.3 = bf16[2048,128]{1,0:T(8,128)(2,1)S(1)} reduce(bf16[2048,1,128]{2,1,0:T(2,128)(2,1)S(1)} %bitcast.157, bf16[]{:T(256)} %broadcast.287), dimensions={1}, to_apply=%bitcast.109.reduce_sub_computation | reduce | bytes 1048578
  43.8 4.9 %all-to-all-start.1 = ((bf16[8,2,16384]{2,1,0:T(2,128)(2,1)}), bf16[8,2,16384]{2,1,0:T(2,128)(2,1)S(1)}, u32[]{:S(2)}, u32[]{:S(2)}) async-start(bf16[8,2,16384]{2,1,0:T(2,128)(2,1)} %reshape.320), calls=%async_computation.1 | async-start | bytes 1048576 | tf_op jit(solution)/shard_map/all_to_all | solution.py:50
  49.5 11.5 %reduce.5 = bf16[2048,128]{1,0:T(8,128)(2,1)S(1)} reduce(bf16[2048,1,128]{2,1,0:T(2,128)(2,1)S(1)} %bitcast.158, bf16[]{:T(256)} %broadcast.287), dimensions={1}, to_apply=%bitcast.111.reduce_sub_computation | reduce | bytes 1048578
  62.8 6.0 %all-to-all-start.2 = ((bf16[8,2,16384]{2,1,0:T(2,128)(2,1)}), bf16[8,2,16384]{2,1,0:T(2,128)(2,1)}, u32[]{:S(2)}, u32[]{:S(2)}) async-start(bf16[8,2,16384]{2,1,0:T(2,128)(2,1)} %reshape.322), calls=%async_computation.2 | async-start | bytes 1048576 | tf_op jit(solution)/shard_map/all_to_all | solution.py:51
  74.7 7.6 %all-to-all-done.2 = bf16[8,2,16384]{2,1,0:T(2,128)(2,1)} async-done(((bf16[8,2,16384]{2,1,0:T(2,128)(2,1)}), bf16[8,2,16384]{2,1,0:T(2,128)(2,1)}, u32[]{:S(2)}, u32[]{:S(2)}) %all-to-all-start.2) | async-done | bytes 524320 | tf_op jit(solution)/shard_map/all_to_all | solution.py:51
  86.5 31.6 %while.10 = (s32[]{:T(128)}, bf16[4,256,2,128]{3,2,1,0:T(2,128)(2,1)S(1)}, bf16[4,256,2,2,64]{1,4,3,2,0:T(8,128)(2,1)S(1)}, bf16[1024,2,2,64]{0,3,2,1:T(8,128)(2...) while((s32[]{:T(128)}, ...), condition=%wide.region_4.5_spmd, body=%wide.region_0.4_spmd.sunk | while | flops 274531840 | bytes 19153508 | solution.py:73
  86.5 3.3 fusion.74
  94.4 3.3 fusion.74
  102.3 3.3 fusion.74
  110.2 3.3 fusion.74
  118.9 3.6 reshape.307
  122.5 3.8 reduce.6
  127.2 3.7 all-to-all-start.3
  131.6 13.1 %all-to-all-done.3 = bf16[8,2,16384]{2,1,0:T(2,128)(2,1)S(1)} async-done(((bf16[8,2,16384]{2,1,0:T(2,128)(2,1)}), bf16[8,2,16384]{2,1,0:T(2,128)(2,1)S(1)}, u32[]{:S(2)}, u32[]{:S(2)}) %all-to-all-start.3) | async-done | bytes 524320 | tf_op jit(solution)/shard_map/all_to_all | solution.py:74
  145.6 4.8 multiply_reduce_fusion.4
  151.6 5.9 %scatter_custom_fusion = bf16[384,2048]{1,0:T(8,128)(2,1)S(1)} fusion(s32[256]{0:T(256)S(1)} %bitcast.164, bf16[128,2048]{1,0:T(8,128)(2,1)S(1)} %fusion.38, s32[1024]{0:T(1024)S(1)} %pad_clamp_fusion.1, bf16[]{:T(256)} %constant.86.clone.1), kind=kCustom, calls=%fused_computation.47 | custom fusion | bytes 1572866 | tf_op jit(solution)/shard_map/scatter | solution.py:101
  157.5 39.8 %all_to_all.58 = bf16[8,48,2048]{2,1,0:T(8,128)(2,1)S(1)} all-to-all(bf16[8,48,2048]{2,1,0:T(8,128)(2,1)S(1)} %bitcast.150), channel_id=1, replica_groups=mesh['sp'=8,'dp'=4] {'sp'}, dimensions={0} | all-to-all | bytes 3145728 | tf_op jit(solution)/shard_map/all_to_all | solution.py:104
  197.3 19.8 %collective-permute-done = bf16[8,1,48,2048]{3,2,1,0:T(8,128)(2,1)S(1)} collective-permute-done((bf16[8,1,48,2048]{3,2,1,0:T(8,128)(2,1)S(1)}, bf16[8,1,48,2048]{3,2,1,0:T(8,128)(2,1)S(1)}, u32[]{:S(2)}, u32[]{:S(2)}) %collective-permute-start) | collective-permute-done | bytes 1572896 | tf_op jit(solution)/shard_map/ppermute | solution.py:109
  217.1 19.9 %collective-permute-done.1 = bf16[8,1,48,2048]{3,2,1,0:T(8,128)(2,1)} collective-permute-done((bf16[8,1,48,2048]{3,2,1,0:T(8,128)(2,1)S(1)}, bf16[8,1,48,2048]{3,2,1,0:T(8,128)(2,1)}, u32[]{:S(2)}, u32[]{:S(2)}) %collective-permute-start.1) | collective-permute-done | bytes 1572896 | tf_op jit(solution)/shard_map/ppermute | solution.py:109
  237.5 20.1 %collective-permute-done.2 = bf16[8,1,48,2048]{3,2,1,0:T(8,128)(2,1)} collective-permute-done((bf16[8,1,48,2048]{3,2,1,0:T(8,128)(2,1)}, bf16[8,1,48,2048]{3,2,1,0:T(8,128)(2,1)}, u32[]{:S(2)}, u32[]{:S(2)}) %collective-permute-start.2) | collective-permute-done | bytes 1572896 | tf_op jit(solution)/shard_map/ppermute | solution.py:109
  257.6 2.8 constant_dynamic-update-slice_fusion.8
  260.4 2.7 constant_dynamic-update-slice_fusion.7
  273.8 3.5 constant_dynamic-slice_fusion.1
  279.9 8.5 %fusion.33 = f32[1536,1024]{1,0:T(8,128)} fusion(bf16[1536,2048]{1,0:T(8,128)(2,1)S(1)} %bitcast.148, bf16[1,2048,1024]{2,1,0:T(8,128)(2,1)S(1)} %copy-done.15), kind=kOutput, calls=%fused_computation.34 | convolution fusion | flops 6442450944 | bytes 16777216 | tf_op jit(solution)/shard_map/dot_general | solution.py:115
  288.4 20.6 %convolution_convert_fusion = bf16[1536,2048]{1,0:T(8,128)(2,1)} fusion(bf16[1,1024,2048]{2,1,0:T(8,128)(2,1)} %param.31, f32[1536,1024]{1,0:T(8,128)} %fusion.33, bf16[1536,2048]{1,0:T(8,128)(2,1)} %bitcast.149, bf16[1,2048,1024]{2,1,0:T(8,128)(2,1)} %param.30), kind=kOutput, calls=%fused_computation.30 | convolution fusion | flops 12897484800 | bytes 27262976 | tf_op jit(solution)/shard_map/dot_general | solution.py:118
  310.3 117.8 %all-reduce.3.cloned.1.call-done = bf16[8,4,48,2048]{3,2,1,0:T(8,128)(2,1)} async-done(((bf16[8,4,48,2048]{3,2,1,0:T(8,128)(2,1)}), bf16[8,4,48,2048]{3,2,1,0:T(8,128)(2,1)}) %all-reduce.3.cloned.1.call-update) | async-done | bytes 6291472
  428.1 3.3 constant_dynamic-slice_fusion
  431.4 5.7 %all-to-all-start.5 = ((bf16[8,1,48,2048]{3,2,1,0:T(8,128)(2,1)}), bf16[8,1,48,2048]{3,2,1,0:T(8,128)(2,1)S(1)}, u32[]{:S(2)}, u32[]{:S(2)}) async-start(bf16[8,1,48,2048]{3,2,1,0:T(8,128)(2,1)} %constant_dynamic-slice_fusion), calls=%async_computation.5 | async-start | bytes 3145728 | tf_op jit(solution)/shard_map/all_to_all | solution.py:126
  437.3 36.4 %all-to-all-done.5 = bf16[8,1,48,2048]{3,2,1,0:T(8,128)(2,1)S(1)} async-done(((bf16[8,1,48,2048]{3,2,1,0:T(8,128)(2,1)}), bf16[8,1,48,2048]{3,2,1,0:T(8,128)(2,1)S(1)}, u32[]{:S(2)}, u32[]{:S(2)}) %all-to-all-start.5) | async-done | bytes 1572896 | tf_op jit(solution)/shard_map/all_to_all | solution.py:126
  478.5 3.2 multiply_reduce_fusion.2
  (135 shorter events, 62.9 us)
Async XLA Ops:
  6.5 22.8 %copy-start.3 = (bf16[1,128,2048]{2,1,0:T(8,128)(2,1)S(1)}, bf16[1,128,2048]{2,1,0:T(8,128)(2,1)}, u32[]{:S(2)}) copy-start(bf16[1,128,2048]{2,1,0:T(8,128)(2,1)} %param.18) | copy-start | bytes 1572868
  9.5 39.2 %copy-start.4 = (bf16[1,128,2048]{2,1,0:T(8,128)(2,1)S(1)}, bf16[1,128,2048]{2,1,0:T(8,128)(2,1)}, u32[]{:S(2)}) copy-start(bf16[1,128,2048]{2,1,0:T(8,128)(2,1)} %param.19) | copy-start | bytes 1572868
  22.0 21.8 %all-to-all-start = ((bf16[8,2,16384]{2,1,0:T(2,128)(2,1)}), bf16[8,2,16384]{2,1,0:T(2,128)(2,1)S(1)}, u32[]{:S(2)}, u32[]{:S(2)}) async-start(bf16[8,2,16384]{2,1,0:T(2,128)(2,1)} %reshape.318), calls=%async_computation | async-start | bytes 1048576 | tf_op jit(solution)/shard_map/all_to_all | solution.py:49
  30.1 31.9 %copy-start.14 = (s32[1,128,2]{1,2,0:T(2,128)S(1)}, s32[1,128,2]{1,2,0:T(2,128)}, u32[]{:S(2)}) copy-start(s32[1,128,2]{1,2,0:T(2,128)} %param.27) | copy-start | bytes 3076
  43.8 19.0 %all-to-all-start.1 = ((bf16[8,2,16384]{2,1,0:T(2,128)(2,1)}), bf16[8,2,16384]{2,1,0:T(2,128)(2,1)S(1)}, u32[]{:S(2)}, u32[]{:S(2)}) async-start(bf16[8,2,16384]{2,1,0:T(2,128)(2,1)} %reshape.320), calls=%async_computation.1 | async-start | bytes 1048576 | tf_op jit(solution)/shard_map/all_to_all | solution.py:50
  62.8 19.5 %all-to-all-start.2 = ((bf16[8,2,16384]{2,1,0:T(2,128)(2,1)}), bf16[8,2,16384]{2,1,0:T(2,128)(2,1)}, u32[]{:S(2)}, u32[]{:S(2)}) async-start(bf16[8,2,16384]{2,1,0:T(2,128)(2,1)} %reshape.322), calls=%async_computation.2 | async-start | bytes 1048576 | tf_op jit(solution)/shard_map/all_to_all | solution.py:51
  69.2 3.6 copy-start.13
  84.6 1.9 copy-start.5
  84.6 1.9 copy-start.8
  84.6 1.9 copy-start.16
  118.1 0.8 copy-start.6
  118.9 12.5 %slice-start = ((s32[8,3]{0,1:T(4,128)}), s32[8,2]{0,1:T(2,128)S(1)}, s32[]{:S(2)}) async-start(s32[8,3]{0,1:T(4,128)} %copy-done.13), calls=%async_computation.7 | async-start | bytes 2048 | tf_op jit(solution)/shard_map/slice.1
  127.2 17.5 %all-to-all-start.3 = ((bf16[8,2,16384]{2,1,0:T(2,128)(2,1)}), bf16[8,2,16384]{2,1,0:T(2,128)(2,1)S(1)}, u32[]{:S(2)}, u32[]{:S(2)}) async-start(bf16[8,2,16384]{2,1,0:T(2,128)(2,1)} %reshape.324), calls=%async_computation.3 | async-start | bytes 1048576 | tf_op jit(solution)/shard_map/all_to_all | solution.py:74
  130.9 297.2 %all-reduce.3.cloned.1.call-start = ((), (), s32[]{:S(2)}) async-start(), calls=%async_computation.6 | async-start | bytes 12582912
  145.6 4.8 copy-start.7
  145.6 4.8 copy-start.10
  145.6 5.2 %copy-start.11 = (f32[2048]{0:T(1024)S(1)}, f32[2048]{0:T(1024)}, u32[]{:S(2)}) copy-start(f32[2048]{0:T(1024)} %param.25) | copy-start | bytes 24580
  150.8 0.8 copy-start.1
  197.3 19.8 %collective-permute-start = (bf16[8,1,48,2048]{3,2,1,0:T(8,128)(2,1)S(1)}, bf16[8,1,48,2048]{3,2,1,0:T(8,128)(2,1)S(1)}, u32[]{:S(2)}, u32[]{:S(2)}) collective-permute-start(bf16[8,1,48,2048]{3,2,1,0:T(8,128)(2,1)S(1)} %bitcast.146), channel_id=1, source_target_pairs={{0,1},{1,2},{2,3},{3,0},{4,5},{5,6},{6,7},{7,4},{8,9},{9,10},{10,1... | collective-permute-start | bytes 4718600 | tf_op jit(solution)/shard_map/ppermute | solution.py:109
  217.1 19.9 %collective-permute-start.1 = (bf16[8,1,48,2048]{3,2,1,0:T(8,128)(2,1)S(1)}, bf16[8,1,48,2048]{3,2,1,0:T(8,128)(2,1)}, u32[]{:S(2)}, u32[]{:S(2)}) collective-permute-start(bf16[8,1,48,2048]{3,2,1,0:T(8,128)(2,1)S(1)} %collective-permute-done), channel_id=1, source_target_pairs={{0,1},{1,2},{2,3},{3,0},{4,5},{5,6},{6,7},{7,4},{8,9},{9,10},{10,1... | collective-permute-start | bytes 4718600 | tf_op jit(solution)/shard_map/ppermute | solution.py:109
  237.1 20.5 %collective-permute-start.2 = (bf16[8,1,48,2048]{3,2,1,0:T(8,128)(2,1)}, bf16[8,1,48,2048]{3,2,1,0:T(8,128)(2,1)}, u32[]{:S(2)}, u32[]{:S(2)}) collective-permute-start(bf16[8,1,48,2048]{3,2,1,0:T(8,128)(2,1)} %collective-permute-done.1), channel_id=1, source_target_pairs={{0,1},{1,2},{2,3},{3,0},{4,5},{5,6},{6,7},{7,4},{8,9},{9,10},{10,1... | collective-permute-start | bytes 4718600 | tf_op jit(solution)/shard_map/ppermute | solution.py:109
  273.8 6.2 %copy-start.15 = (bf16[1,2048,1024]{2,1,0:T(8,128)(2,1)S(1)}, bf16[1,2048,1024]{2,1,0:T(8,128)(2,1)}, u32[]{:S(2)}) copy-start(bf16[1,2048,1024]{2,1,0:T(8,128)(2,1)} %param.29) | copy-start | bytes 12582916
  277.3 2.6 copy-start
  309.0 0.7 copy-start.17
  309.0 128.1 %copy-start.9 = (f32[1,128,2]{1,2,0:T(2,128)S(1)}, f32[1,128,2]{1,2,0:T(2,128)}, u32[]{:S(2)}) copy-start(f32[1,128,2]{1,2,0:T(2,128)} %param.28) | copy-start | bytes 3076
  431.4 42.3 %all-to-all-start.5 = ((bf16[8,1,48,2048]{3,2,1,0:T(8,128)(2,1)}), bf16[8,1,48,2048]{3,2,1,0:T(8,128)(2,1)S(1)}, u32[]{:S(2)}, u32[]{:S(2)}) async-start(bf16[8,1,48,2048]{3,2,1,0:T(8,128)(2,1)} %constant_dynamic-slice_fusion), calls=%async_computation.5 | async-start | bytes 3145728 | tf_op jit(solution)/shard_map/all_to_all | solution.py:126
  476.1 5.8 %copy-start.2 = (bf16[128,2048]{1,0:T(8,128)(2,1)S(1)}, bf16[128,2048]{1,0:T(8,128)(2,1)}, u32[]{:S(2)}) copy-start(bf16[128,2048]{1,0:T(8,128)(2,1)} %copy-done.1) | copy-start | bytes 1572868
  476.1 5.8 %copy-start.12 = (f32[2048]{0:T(1024)S(1)}, f32[2048]{0:T(1024)}, u32[]{:S(2)}) copy-start(f32[2048]{0:T(1024)} %param.26) | copy-start | bytes 24580
Sparse Core Ops, SparseCore 0:
  309.2 118.8 all-reduce.2
